TPU v7x, 32 devices: a whole 2x2x4 slice. The times are simulated.
32 devices in a mesh: dp: 4 (over y, x), kv: 4 (over z), tp: 2 (over core).
Axes of the slice: x: 2, y: 2, z: 4, core: 2. Of those that a mesh axis runs over, the one named last changes fastest.
Arguments:
- residual: bfloat16 [32, 2048], P('dp', ('kv', 'tp')), may hold values from -6 to 6
- norm_gains: float32 [3, 2048], replicated, may hold values from 0.1 to 1.9
- ffn_gate: bfloat16 [2, 5632, 2048], P(None, ('kv', 'tp')), may hold values from -0.125 to 0.125
- ffn_up: bfloat16 [2, 5632, 2048], P(None, ('kv', 'tp')), may hold values from -0.125 to 0.125
- ffn_down: bfloat16 [2, 5632, 2048], P(None, ('kv', 'tp')), may hold values from -0.1875 to 0.1875
- proj_query: bfloat16 [2048, 1024], P('kv', 'tp'), may hold values from -0.44194174 to 0.44194174
- proj_key: bfloat16 [2048, 256], P('kv', 'tp'), may hold values from -0.125 to 0.125
- proj_value: bfloat16 [2048, 256], P('kv', 'tp'), may hold values from -0.125 to 0.125
- proj_out: bfloat16 [1024, 2048], P('tp', 'kv'), may hold values from -0.1875 to 0.1875
- head_lambda: float32 [8], P('tp'), may hold values from 0.3 to 0.8
- head_gain: float32 [128], replicated, may hold values from 0.1 to 1.9
- cache_keys: bfloat16 [32, 1024, 2, 128], P('dp', 'kv', 'tp'), may hold values from -12 to 12
- cache_values: bfloat16 [32, 1024, 2, 128], P('dp', 'kv', 'tp'), may hold values from -6 to 6
- live_length: int32 [32], P('dp'), may hold values from 1 to 1024, 8192 in all
Outputs:
- updated: bfloat16 [32, 2048], P('dp', ('kv', 'tp'))
Inputs may be any that keep to these rules, and one draw needn't show every extreme that they name: `live_length`: the largest length of every draw equals 1024.
All inputs are finite; a program needn't handle non-finite values. No bound on the sum of `live_length` on one device may be relied on, other than what follows from the above.
Results may differ from a plain program's by a relative error of at most 0.014.
The roundings to bfloat16 on the way count: a program that leaves them out, or rounds other values in their place, can miss the bound.
Values may be sent and summed in bfloat16 or wider, within the bound.
A program may use at most 64 MiB of HBM per device.

v0:
```python
import jax
import jax.numpy as jnp
from jax import lax
from jax.sharding import PartitionSpec as P

D = 2048
HEAD = 64
VDIM = 128


epsilon = 1e-05


def joined(part, axis, combine):
    gathered = jax.tree.map(lambda a: lax.all_gather(a, axis), part)

    def take(source):
        return jax.tree.map(lambda a: lax.dynamic_index_in_dim(a, source, 0, False), gathered)

    return lax.fori_loop(
        1, lax.axis_size(axis), lambda source, state: combine(state, take(source)), take(0)
    )


def row_scale(row_data):
    data32 = row_data.astype(jnp.float32)
    return lax.rsqrt(jnp.mean(data32 * data32, axis=-1, keepdims=True) + epsilon)


def channel_mix(row_data, gain, gate_part, up_part, down_part):
    normed = (row_data.astype(jnp.float32) * row_scale(row_data) * gain).astype(jnp.bfloat16)
    contract = (((1,), (1,)), ((), ()))
    gate_act = lax.dot_general(normed, gate_part, contract, preferred_element_type=jnp.float32)
    up_act = lax.dot_general(normed, up_part, contract, preferred_element_type=jnp.float32)
    hidden = (jax.nn.silu(gate_act) * up_act).astype(jnp.bfloat16)
    return 0.5 * jnp.dot(hidden, down_part, preferred_element_type=jnp.float32)


def join_parts(earlier, latter):
    highest = jnp.maximum(earlier[0], latter[0])
    weight_early = jnp.exp(earlier[0] - highest)
    weight_late = jnp.exp(latter[0] - highest)
    return (
        highest,
        earlier[1] * weight_early + latter[1] * weight_late,
        earlier[2] * weight_early[..., None] + latter[2] * weight_late[..., None],
    )


def local(
    residual,
    norm_gains,
    ffn_gate,
    ffn_up,
    ffn_down,
    proj_query,
    proj_key,
    proj_value,
    proj_out,
    head_lambda,
    head_gain,
    cache_keys,
    cache_values,
    live_length,
):
    rows_one = lax.all_gather(residual, ("kv", "tp"), axis=1, tiled=True)
    term_one = channel_mix(rows_one, norm_gains[0], ffn_gate[0], ffn_up[0], ffn_down[0])
    kv_place = lax.axis_index("kv")
    block_width = proj_query.shape[0]
    summed = lax.psum_scatter(term_one, ("kv", "tp"), scatter_dimension=1, tiled=True)
    stream_own = (residual.astype(jnp.float32) + summed).astype(jnp.bfloat16)
    row_block = lax.all_gather(stream_own, "tp", axis=1, tiled=True)
    gain_block = lax.dynamic_slice_in_dim(norm_gains[1], kv_place * block_width, block_width, 0)
    block_data = row_block.astype(jnp.float32)
    squares = jnp.sum(block_data * block_data, axis=1)
    scaled = (block_data * gain_block).astype(jnp.bfloat16)
    query_part = jnp.dot(scaled, proj_query, preferred_element_type=jnp.float32)
    key_part = jnp.dot(scaled, proj_key, preferred_element_type=jnp.float32)
    value_part = jnp.dot(scaled, proj_value, preferred_element_type=jnp.float32)
    queries, key_new, value_new, square_sum = lax.psum(
        (query_part, key_part, value_part, squares), "kv"
    )
    factor = lax.rsqrt(square_sum / D + epsilon)[:, None]
    batch_rows = residual.shape[0]
    kv_local = key_new.shape[1] // (2 * HEAD)
    group_size = queries.shape[1] // (2 * HEAD * kv_local)
    queries = (
        (queries * factor).astype(jnp.bfloat16).reshape(batch_rows, kv_local, group_size, 2, HEAD)
    )
    key_new = (key_new * factor).astype(jnp.bfloat16).reshape(batch_rows, kv_local, 2, HEAD)
    value_new = (value_new * factor).astype(jnp.bfloat16).reshape(batch_rows, kv_local, VDIM)
    span = cache_keys.shape[1]
    block_keys = cache_keys.reshape(batch_rows, span, kv_local, 2, HEAD)
    score_scale = HEAD ** (-0.5)
    scores = (
        jnp.einsum("bkgcd,bpkcd->bkgcp", queries, block_keys, preferred_element_type=jnp.float32)
        * score_scale
    )
    positions = kv_place * span + jnp.arange(span, dtype=jnp.int32)
    live_mask = (positions[None, :] < live_length[:, None])[:, None, None, None, :]
    highest = jnp.max(jnp.where(live_mask, scores, -1e30), axis=-1)
    exp_terms = jnp.where(live_mask, jnp.exp(scores - highest[..., None]), 0.0)
    totals = jnp.sum(exp_terms, axis=-1)
    weights = exp_terms.astype(jnp.bfloat16)
    partial_value = jnp.einsum(
        "bkgcp,bpkv->bkgcv", weights, cache_values, preferred_element_type=jnp.float32
    )
    running = joined((highest, totals, partial_value), "kv", join_parts)
    lead_shape = totals.shape
    own_scores = (
        jnp.einsum("bkgcd,bkcd->bkgc", queries, key_new, preferred_element_type=jnp.float32)
        * score_scale
    )
    own_values = jnp.broadcast_to(
        value_new.astype(jnp.float32)[:, :, None, None, :], lead_shape + (VDIM,)
    )
    highest, totals, accum = join_parts(
        running, (own_scores, jnp.ones(lead_shape, jnp.float32), own_values)
    )
    ratios = accum / totals[..., None]
    lambdas = head_lambda.reshape(kv_local, group_size)
    mixed_heads = ratios[:, :, :, 0] - lambdas[None, :, :, None] * ratios[:, :, :, 1]
    heads_out = (mixed_heads * row_scale(mixed_heads) * head_gain).astype(jnp.bfloat16)
    heads_out = heads_out.reshape(batch_rows, kv_local * group_size * VDIM)
    out_part = jnp.dot(heads_out, proj_out, preferred_element_type=jnp.float32)
    mixer_out = lax.psum_scatter(out_part, "tp", scatter_dimension=1, tiled=True)
    stream_two = (stream_own.astype(jnp.float32) + mixer_out).astype(jnp.bfloat16)
    rows_two = lax.all_gather(stream_two, ("kv", "tp"), axis=1, tiled=True)
    term_two = channel_mix(rows_two, norm_gains[2], ffn_gate[1], ffn_up[1], ffn_down[1])
    summed_two = lax.psum_scatter(term_two, ("kv", "tp"), scatter_dimension=1, tiled=True)
    return (stream_two.astype(jnp.float32) + summed_two).astype(jnp.bfloat16)


def solution(mesh):
    in_specs = (
        P("dp", ("kv", "tp")),
        P(),
        P(None, ("kv", "tp"), None),
        P(None, ("kv", "tp"), None),
        P(None, ("kv", "tp"), None),
        P("kv", "tp"),
        P("kv", "tp"),
        P("kv", "tp"),
        P("tp", "kv"),
        P("tp"),
        P(),
        P("dp", "kv", "tp", None),
        P("dp", "kv", "tp", None),
        P("dp"),
    )
    out_specs = P("dp", ("kv", "tp"))
    return jax.shard_map(local, mesh=mesh, in_specs=in_specs, out_specs=out_specs, check_vma=False)
```

profile of v0, /device:TPU:0, one launch (start us, length us, event | category | flops | bytes accessed | tf_op | source)
XLA Modules:
  0.0 196.0 jit_solution(17430389312642090075)
XLA Ops:
  6.6 16.1 %all_gather.27 = bf16[8,2048]{1,0:T(8,128)(2,1)S(1)} all-gather(bf16[8,256]{1,0:T(8,128)(2,1)} %param.16), channel_id=1, replica_groups=mesh['dp'=4,'kv'=4,'tp'=2] {'kv','tp'}, dimensions={1}, use_global_device_ids=true | all-gather | bytes 36864 | tf_op jit(solution)/shard_map/all_gather | solution.py:66
  22.8 0.9 fusion.108
  23.7 2.7 %fusion.16 = f32[8,704]{1,0:T(8,128)S(1)} fusion(bf16[2,704,2048]{2,1,0:T(8,128)(2,1)} %param.18, bf16[8,2048]{1,0:T(8,128)(2,1)S(1)} %all_gather.27, f32[2048]{0:T(1024)S(1)} %bitcast.170, f32[8]{0:T(128)S(1)} %add_rsqrt_fusion.3), kind=kOutput, calls=%fused_computation.22 | convolution fusion | flops 23134208 | bytes 2947104 | tf_op jit(solution)/shard_map/dot_general | solution.py:33
  26.4 5.0 %fusion.24 = f32[8,2048]{1,0:T(8,128)} fusion(bf16[2,704,2048]{2,1,0:T(8,128)(2,1)} %param.20, bf16[2,704,2048]{2,1,0:T(8,128)(2,1)} %param.19, f32[8,704]{1,0:T(8,128)S(1)} %fusion.16, bf16[8,2048]{1,0:T(8,128)(2,1)S(1)} %all_gather.27, f32[2048]{0:T(1024)S(1)} %bitcast.171, f32[8]{0:T(128)S(1)} %add_rsqrt_fusion.3), kind=kOutput, calls=%fused_computation.30 | convolution fusion | flops 46253056 | bytes 5896224 | tf_op jit(solution)/shard_map/dot_general | solution.py:36
  32.0 31.1 %reduce-scatter.4.cloned.1.call-done = f32[8,256]{1,0:T(8,128)} async-done(((f32[8,2048]{1,0:T(8,128)}), f32[8,256]{1,0:T(8,128)}) %reduce-scatter.4.cloned.1.call-update) | async-done | bytes 8208 | tf_op jit(solution)/shard_map/reduce_scatter | solution.py:70
  63.1 0.7 add_convert_fusion.2
  63.8 1.8 all_gather.28
  66.2 15.8 %all-reduce = (f32[8,512]{1,0:T(8,128)S(1)}, f32[8]{0:T(128)S(1)}, f32[8,128]{1,0:T(8,128)S(1)}, f32[8,128]{1,0:T(8,128)S(1)}) all-reduce(f32[8,512]{1,0:T(8,128)S(1)} %fusion.98, f32[8]{0:T(128)S(1)} %fusion.73, f32[8,128]{1,0:T(8,128)S(1)} %fusion.96, f32[8,128]{1,0:T(8,128)S(1)} %fusion.94), channel_id=1, replica_groups=mesh['dp'=4,'kv'=4,'tp'=2] {'kv'}, use_global_device_ids=true, to_apply=%region_2.3 | all-reduce | flops 6152 | bytes 49216 | tf_op jit(solution)/shard_map/psum | solution.py:80
  82.5 0.3 select_reduce_fusion
  82.8 13.1 %all-gather = f32[32,4,2]{1,2,0:T(2,128)S(1)} all-gather(f32[8,4,2]{1,2,0:T(2,128)S(1)} %get-tuple-element.240), channel_id=2, replica_groups=mesh['dp'=4,'kv'=4,'tp'=2] {'kv'}, dimensions={0}, use_global_device_ids=true | all-gather | bytes 1280 | tf_op jit(solution)/shard_map/all_gather | solution.py:15
  96.1 0.3 fusion.47
  96.4 13.3 %all-gather.2 = f32[32,4,2,128]{3,1,2,0:T(4,128)S(1)} all-gather(f32[8,4,2,128]{3,1,2,0:T(4,128)S(1)} %fusion.47), channel_id=4, replica_groups=mesh['dp'=4,'kv'=4,'tp'=2] {'kv'}, dimensions={0}, use_global_device_ids=true | all-gather | bytes 163840 | tf_op jit(solution)/shard_map/all_gather | solution.py:15
  109.8 13.1 %all-gather.1 = f32[32,4,2]{1,2,0:T(2,128)S(1)} all-gather(f32[8,4,2]{1,2,0:T(2,128)S(1)} %fusion.56), channel_id=3, replica_groups=mesh['dp'=4,'kv'=4,'tp'=2] {'kv'}, dimensions={0}, use_global_device_ids=true | all-gather | bytes 1280 | tf_op jit(solution)/shard_map/all_gather | solution.py:15
  123.3 1.6 while.19
  123.6 0.2 fusion.121
  124.1 0.2 fusion.121
  125.7 0.8 fusion.83
  126.6 7.2 %reduce-scatter.6.cloned.1.call-done = f32[8,256]{1,0:T(8,128)} async-done(((f32[8,512]{1,0:T(8,128)}), f32[8,256]{1,0:T(8,128)}) %reduce-scatter.6.cloned.1.call-update) | async-done | bytes 8208 | tf_op jit(solution)/shard_map/reduce_scatter | solution.py:126
  133.9 0.7 add_convert_fusion.1
  134.6 14.3 %all_gather.35 = bf16[8,2048]{1,0:T(8,128)(2,1)S(1)} all-gather(bf16[8,256]{1,0:T(8,128)(2,1)S(1)} %add_convert_fusion.1), channel_id=1, replica_groups=mesh['dp'=4,'kv'=4,'tp'=2] {'kv','tp'}, dimensions={1}, use_global_device_ids=true | all-gather | bytes 36864 | tf_op jit(solution)/shard_map/all_gather | solution.py:128
  149.0 2.7 %fusion.10 = f32[8,704]{1,0:T(8,128)S(1)} fusion(bf16[2,704,2048]{2,1,0:T(8,128)(2,1)} %param.18, bf16[8,2048]{1,0:T(8,128)(2,1)S(1)} %all_gather.35, f32[2048]{0:T(1024)S(1)} %bitcast.168, f32[8]{0:T(128)S(1)} %add_rsqrt_fusion.1), kind=kOutput, calls=%fused_computation.16 | convolution fusion | flops 23134208 | bytes 2947104 | tf_op jit(solution)/shard_map/dot_general | solution.py:33
  151.7 5.0 %fusion.27 = f32[8,2048]{1,0:T(8,128)} fusion(bf16[2,704,2048]{2,1,0:T(8,128)(2,1)} %param.20, bf16[2,704,2048]{2,1,0:T(8,128)(2,1)} %param.19, f32[8,704]{1,0:T(8,128)S(1)} %fusion.10, bf16[8,2048]{1,0:T(8,128)(2,1)S(1)} %all_gather.35, f32[2048]{0:T(1024)S(1)} %bitcast.169, f32[8]{0:T(128)S(1)} %add_rsqrt_fusion.1), kind=kOutput, calls=%fused_computation.31 | convolution fusion | flops 46253056 | bytes 5896224 | tf_op jit(solution)/shard_map/dot_general | solution.py:36
  156.7 31.5 %reduce-scatter.8.cloned.1.call-done = f32[8,256]{1,0:T(8,128)} async-done(((f32[8,2048]{1,0:T(8,128)}), f32[8,256]{1,0:T(8,128)}) %reduce-scatter.8.cloned.1.call-update) | async-done | bytes 8208 | tf_op jit(solution)/shard_map/reduce_scatter | solution.py:130
  188.2 1.3 add_convert_fusion
  (83 shorter events, 4.4 us)
Async XLA Ops:
  6.5 89.6 %copy-start = (bf16[8,256,1,128]{3,1,2,0:T(8,128)(2,1)S(1)}, bf16[8,256,1,128]{3,1,2,0:T(8,128)(2,1)}, u32[]{:S(2)}) copy-start(bf16[8,256,1,128]{3,1,2,0:T(8,128)(2,1)} %param.28) | copy-start | bytes 1572868
  6.5 56.6 %copy-start.6 = (bf16[8,256]{1,0:T(8,128)(2,1)S(1)}, bf16[8,256]{1,0:T(8,128)(2,1)}, u32[]{:S(2)}) copy-start(bf16[8,256]{1,0:T(8,128)(2,1)} %param.16) | copy-start | bytes 12292
  6.5 25.0 %copy-start.7 = (f32[4]{0:T(128)S(1)}, f32[4]{0:T(128)}, u32[]{:S(2)}) copy-start(f32[4]{0:T(128)} %param.25) | copy-start | bytes 52
  6.5 25.0 %copy-start.8 = (f32[128]{0:T(128)S(1)}, f32[128]{0:T(128)}, u32[]{:S(2)}) copy-start(f32[128]{0:T(128)} %param.26) | copy-start | bytes 1540
  6.5 25.1 %copy-start.9 = (s32[8]{0:T(128)S(1)}, s32[8]{0:T(128)}, u32[]{:S(2)}) copy-start(s32[8]{0:T(128)} %param.29) | copy-start | bytes 100
  6.5 25.2 %copy-start.1 = (bf16[8,256,1,128]{3,1,2,0:T(8,128)(2,1)S(1)}, bf16[8,256,1,128]{3,1,2,0:T(8,128)(2,1)}, u32[]{:S(2)}) copy-start(bf16[8,256,1,128]{3,1,2,0:T(8,128)(2,1)} %param.27) | copy-start | bytes 1572868
  6.6 59.2 %copy-start.2 = (bf16[512,512]{1,0:T(8,128)(2,1)S(1)}, bf16[512,512]{1,0:T(8,128)(2,1)}, u32[]{:S(2)}) copy-start(bf16[512,512]{1,0:T(8,128)(2,1)} %param.21) | copy-start | bytes 1572868
  6.6 59.3 %copy-start.4 = (bf16[512,128]{1,0:T(8,128)(2,1)S(1)}, bf16[512,128]{1,0:T(8,128)(2,1)}, u32[]{:S(2)}) copy-start(bf16[512,128]{1,0:T(8,128)(2,1)} %param.23) | copy-start | bytes 393220
  6.6 59.5 %copy-start.5 = (bf16[512,128]{1,0:T(8,128)(2,1)S(1)}, bf16[512,128]{1,0:T(8,128)(2,1)}, u32[]{:S(2)}) copy-start(bf16[512,128]{1,0:T(8,128)(2,1)} %param.22) | copy-start | bytes 393220
  6.6 56.5 %reduce-scatter.4.cloned.1.call-start = ((), (), s32[]{:S(2)}) async-start(), calls=%async_computation.3 | async-start | bytes 73728 | tf_op jit(solution)/shard_map/reduce_scatter | solution.py:70
  26.4 99.3 %copy-start.3 = (bf16[512,512]{1,0:T(8,128)(2,1)S(1)}, bf16[512,512]{1,0:T(8,128)(2,1)}, u32[]{:S(2)}) copy-start(bf16[512,512]{1,0:T(8,128)(2,1)} %param.24) | copy-start | bytes 1572868
  31.5 102.4 %reduce-scatter.6.cloned.1.call-start = ((), (), s32[]{:S(2)}) async-start(), calls=%async_computation.4 | async-start | bytes 24576 | tf_op jit(solution)/shard_map/reduce_scatter | solution.py:126
  126.6 61.6 %reduce-scatter.8.cloned.1.call-start = ((), (), s32[]{:S(2)}) async-start(), calls=%async_computation.5 | async-start | bytes 73728 | tf_op jit(solution)/shard_map/reduce_scatter | solution.py:130
Sparse Core Ops, SparseCore 0:
  31.6 31.4 reduce-scatter.3
  126.7 7.1 reduce-scatter.5
  156.8 31.2 reduce-scatter.7
where the time goes:
time: 196 us
  blocking collectives  87.6 us (45%)
  waiting for transfers between devices  69.9 us (36%)
  matrix products  17.3 us (9%)
  between operations  13.3 us (7%)
  other arithmetic  4.66 us (2%)
  local copies, waits for them, and re-layouts  3.08 us (2%)
    all_gather x3, blocking collectives, joined(): gathered = jax.tree.map(lambda a: lax.all_gather(a, axis), part)  39.6 us
    reduce_scatter x1, waiting for transfers between devices, local(): lax.psum_scatter(term_two, ('kv', 'tp'), scatter_dimension=1, tiled=True)  31.5 us
    reduce_scatter x1, waiting for transfers between devices, local(): lax.psum_scatter(term_one, ('kv', 'tp'), scatter_dimension=1, tiled=True)  31.1 us
    all_gather x1, blocking collectives, local(): rows_one = lax.all_gather(residual, ('kv', 'tp'), axis=1, tiled=True)  16.1 us
    psum x1, blocking collectives, local(): lax.psum((query_part, key_part, value_part, squares), 'kv')  15.8 us
    all_gather x1, blocking collectives, local(): rows_two = lax.all_gather(stream_two, ('kv', 'tp'), axis=1, tiled=True)  14.3 us
    dot_general x2, matrix products, channel_mix(): return 0.5 * jnp.dot(hidden, down_part, preferred_element_type=jnp.float32)  10 us
    reduce_scatter x1, waiting for transfers between devices, local(): lax.psum_scatter(out_part, 'tp', scatter_dimension=1, tiled=True)  7.22 us
  transfers between devices with their start and end apart: 3, of which 3 were waited for; matrix products, arithmetic and copies ran while one was open for 0% of the time, Pallas kernels for 0%

commit v1 on v0

--- a/solution.py
+++ b/solution.py
@@ -1,6 +1,10 @@
+import functools
+
 import jax
 import jax.numpy as jnp
 from jax import lax
+from jax.experimental import pallas as pl
+from jax.experimental.pallas import tpu as pltpu
 from jax.sharding import PartitionSpec as P
 
 D = 2048
@@ -131,6 +135,458 @@
     return (stream_two.astype(jnp.float32) + summed_two).astype(jnp.bfloat16)
 
 
+MESH = pl.DeviceIdType.MESH
+NT = (((1,), (1,)), ((), ()))
+SUM_ONE = jnp.float32
+SUM_TWO = jnp.bfloat16
+ATT_TYPE = jnp.float32
+
+
+def fused_kernel(
+    K,
+    T,
+    head_lambda,
+    live_length,
+    residual,
+    norm_gains,
+    ffn_gate,
+    ffn_up,
+    ffn_down,
+    proj_query,
+    proj_key,
+    proj_value,
+    proj_out,
+    head_gain,
+    cache_keys,
+    cache_values,
+    out_ref,
+    gains,
+    gate,
+    up,
+    down,
+    wq,
+    wk,
+    wv,
+    wo,
+    hgain,
+    keys,
+    values,
+    rows_one,
+    send_one,
+    recv_one,
+    stream,
+    qkv,
+    q_rows,
+    att_value,
+    att_stat,
+    ratio_rows,
+    out_parts,
+    rows_two,
+    send_two,
+    recv_two,
+    load_sem,
+    rows_sems,
+    one_sems,
+    qkv_sems,
+    att_sems,
+    out_sems,
+    two_rows_sems,
+    two_sems,
+    lam_ref,
+    len_ref,
+):
+    kv, tp = lax.axis_index("kv"), lax.axis_index("tp")
+    G = K * T
+    me = kv * T + tp
+    B, C = rows_one.shape[1:]
+    W = T * C
+    width = G * C
+
+    def at(dk, dt):
+        return lax.rem(kv + dk, K), lax.rem(tp + dt, T)
+
+    def send(src, dst, sems, lane, slot, place):
+        copy = pltpu.make_async_remote_copy(
+            src_ref=src,
+            dst_ref=dst,
+            send_sem=sems.at[0, lane],
+            recv_sem=sems.at[1, slot],
+            device_id={"kv": place[0], "tp": place[1]},
+            device_id_type=MESH,
+        )
+        copy.start()
+        return copy
+
+    def arrive(dst, sems, slot, place):
+        pltpu.make_async_remote_copy(
+            src_ref=dst,
+            dst_ref=dst,
+            send_sem=sems.at[0, 0],
+            recv_sem=sems.at[1, slot],
+            device_id={"kv": place[0], "tp": place[1]},
+            device_id_type=MESH,
+        ).wait_recv()
+
+    sent = []
+    loads = {}
+
+    def load(name, src, dst):
+        copy = pltpu.make_async_copy(src, dst, load_sem.at[len(loads)])
+        copy.start()
+        loads[name] = copy
+
+    load("rows", residual, rows_one.at[me])
+    barrier = pltpu.get_barrier_semaphore()
+    kv_offsets = sorted(range(1, K), key=lambda dk: abs(2 * dk - K)) + [0]
+    offsets = [(dk, dt) for dk in kv_offsets for dt in range(T)]
+    peers = [o for o in offsets if o != (0, 0)]
+    for dk, dt in peers:
+        k, t = at(dk, dt)
+        pl.semaphore_signal(barrier, inc=1, device_id={"kv": k, "tp": t}, device_id_type=MESH)
+    load("gains", norm_gains, gains)
+    load("gate0", ffn_gate.at[0], gate.at[0])
+    load("up0", ffn_up.at[0], up.at[0])
+    load("down0", ffn_down.at[0], down.at[0])
+    loads["rows"].wait()
+    pl.semaphore_wait(barrier, G - 1)
+    for dk, dt in peers:
+        sent.append(
+            send(rows_one.at[me], rows_one.at[me], rows_sems, dk * T + dt, me, at(dk, dt))
+        )
+    load("wq", proj_query, wq)
+    load("wk", proj_key, wk)
+    load("wv", proj_value, wv)
+    load("wo", proj_out, wo)
+    load("hgain", head_gain, hgain)
+    load("keys", cache_keys, keys)
+    load("values", cache_values, values)
+    load("lam", head_lambda, lam_ref)
+    load("len", live_length, len_ref)
+    load("gate1", ffn_gate.at[1], gate.at[1])
+    load("up1", ffn_up.at[1], up.at[1])
+    load("down1", ffn_down.at[1], down.at[1])
+    loads["gains"].wait()
+    loads["gate0"].wait()
+    loads["up0"].wait()
+    loads["down0"].wait()
+    for dk, dt in peers:
+        k, t = at(dk, dt)
+        arrive(rows_one.at[k * T + t], rows_sems, k * T + t, (k, t))
+
+    def hidden_of(row_data, j, half):
+        data32 = row_data.astype(jnp.float32)
+        scale = lax.rsqrt(jnp.mean(data32 * data32, axis=-1, keepdims=True) + epsilon)
+        normed = (data32 * scale * gains[j : j + 1, :]).astype(jnp.bfloat16)
+        gate_act = lax.dot_general(normed, gate[half], NT, preferred_element_type=jnp.float32)
+        up_act = lax.dot_general(normed, up[half], NT, preferred_element_type=jnp.float32)
+        return (jax.nn.silu(gate_act) * up_act).astype(jnp.bfloat16)
+
+    def down_block(hidden, half, k):
+        block = down[half, :, pl.ds(pl.multiple_of(k * W, W), W)]
+        return 0.5 * jnp.dot(hidden, block, preferred_element_type=jnp.float32)
+
+    with jax.named_scope("half_one"):
+        hidden = hidden_of(jnp.concatenate([rows_one[g] for g in range(G)], axis=1), 0, 0)
+        for dk in kv_offsets:
+            k, _ = at(dk, 0)
+            part = down_block(hidden, 0, k).astype(SUM_ONE)
+            if dk == 0:
+                source = recv_one.at[me]
+                recv_one[me] = part
+            else:
+                source = send_one.at[dk]
+                send_one[dk] = part
+            for dt in range(T):
+                if (dk, dt) != (0, 0):
+                    sent.append(
+                        send(source, recv_one.at[me], one_sems, dk * T + dt, me, at(dk, dt))
+                    )
+        loads["wq"].wait()
+        loads["wk"].wait()
+        loads["wv"].wait()
+        for dk, dt in peers:
+            k, t = at(dk, dt)
+            arrive(recv_one.at[k * T + t], one_sems, k * T + t, (k, t))
+    with jax.named_scope("project"):
+        summed = recv_one[0].astype(jnp.float32)
+        for g in range(1, G):
+            summed = summed + recv_one[g].astype(jnp.float32)
+        base = jnp.concatenate([rows_one[kv * T + t] for t in range(T)], axis=1)
+        stream_one = (base.astype(jnp.float32) + summed).astype(jnp.bfloat16)
+        one32 = stream_one.astype(jnp.float32)
+        stream[...] = one32
+        squares = jnp.sum(one32 * one32, axis=1, keepdims=True)
+        gain_block = gains[1:2, pl.ds(pl.multiple_of(kv * W, W), W)]
+        scaled = (one32 * gain_block).astype(jnp.bfloat16)
+        NQ, NK, NV = wq.shape[1], wk.shape[1], wv.shape[1]
+        qkv[kv] = jnp.concatenate(
+            [
+                jnp.dot(scaled, wq[...], preferred_element_type=jnp.float32),
+                jnp.dot(scaled, wk[...], preferred_element_type=jnp.float32),
+                jnp.dot(scaled, wv[...], preferred_element_type=jnp.float32),
+                jnp.broadcast_to(squares, (B, 128)),
+            ],
+            axis=1,
+        )
+        for dk in kv_offsets[:-1]:
+            sent.append(send(qkv.at[kv], qkv.at[kv], qkv_sems, dk, kv, at(dk, 0)))
+        loads["keys"].wait()
+        loads["values"].wait()
+        loads["lam"].wait()
+        loads["len"].wait()
+        loads["hgain"].wait()
+        loads["wo"].wait()
+        for dk in kv_offsets[:-1]:
+            k, _ = at(dk, 0)
+            arrive(qkv.at[k], qkv_sems, k, (k, tp))
+    with jax.named_scope("attend"):
+        total = qkv[0]
+        for k in range(1, K):
+            total = total + qkv[k]
+        factor = lax.rsqrt(total[:, NQ + NK + NV : NQ + NK + NV + 1] / width + epsilon)
+        queries = (total[:, :NQ] * factor).astype(jnp.bfloat16).astype(jnp.float32)
+        key_new = (total[:, NQ : NQ + NK] * factor).astype(jnp.bfloat16).astype(jnp.float32)
+        value_new = (total[:, NQ + NK : NQ + NK + NV] * factor).astype(jnp.bfloat16)
+        value_new = value_new.astype(jnp.float32)
+        groups = NQ // NK
+        R = 2 * groups
+        lane = lax.broadcasted_iota(jnp.int32, (B, NK), 1)
+        for g in range(groups):
+            head = queries[:, g * NK : (g + 1) * NK]
+            for c in range(2):
+                mine = (lane < NK // 2) if c == 0 else (lane >= NK // 2)
+                q_rows[(g * 2 + c) * B : (g * 2 + c + 1) * B, :] = jnp.where(mine, head, 0.0)
+        score_scale = HEAD ** (-0.5)
+        span = keys.shape[1]
+        q_all, score_list, mask_list = [], [], []
+        position = lax.broadcasted_iota(jnp.int32, (R, span), 1) + kv * span
+        for b in range(B):
+            q_one = q_rows[pl.ds(b, R, stride=B), :]
+            q_all.append(q_one)
+            score_list.append(
+                lax.dot_general(
+                    q_one.astype(jnp.bfloat16), keys[b], NT, preferred_element_type=jnp.float32
+                )
+                * score_scale
+            )
+            mask_list.append(jnp.where(position < len_ref[b], 1.0, 0.0))
+        scores = jnp.concatenate(score_list, axis=0)
+        live = jnp.concatenate(mask_list, axis=0) > 0.5
+        highest = jnp.max(jnp.where(live, scores, -1e30), axis=-1, keepdims=True)
+        exp_terms = jnp.where(live, jnp.exp(scores - highest), 0.0)
+        totals = jnp.sum(exp_terms, axis=-1, keepdims=True)
+        weighted = [
+            jnp.dot(
+                exp_terms[b * R : (b + 1) * R].astype(jnp.bfloat16),
+                values[b],
+                preferred_element_type=jnp.float32,
+            )
+            for b in range(B)
+        ]
+        N = B * R
+        VD = values.shape[2]
+        lanes = lax.broadcasted_iota(jnp.int32, (N, 128), 1)
+        place = lax.rem(lax.broadcasted_iota(jnp.int32, (N, 128), 0), R)
+        high_at, total_at = lanes == place, lanes == place + R
+        packed = jnp.where(high_at, highest, jnp.where(total_at, totals, 0.0))
+        att_stat[kv] = jnp.sum(packed.reshape(B, R, 128), axis=1)
+        att_value[kv] = jnp.concatenate(weighted, axis=0).astype(ATT_TYPE)
+        for dk in kv_offsets[:-1]:
+            sent.append(send(att_stat.at[kv], att_stat.at[kv], att_sems, dk, kv, at(dk, 0)))
+            sent.append(
+                send(att_value.at[kv], att_value.at[kv], att_sems, K + dk, K + kv, at(dk, 0))
+            )
+
+        def wide(a):
+            return jnp.broadcast_to(a[:, None, :], (B, R, a.shape[1])).reshape(N, a.shape[1])
+
+        own_score = jnp.sum(
+            jnp.concatenate(q_all, axis=0) * wide(key_new), axis=-1, keepdims=True
+        ) * score_scale
+        own_value = wide(value_new)
+        for dk in kv_offsets[:-1]:
+            k, _ = at(dk, 0)
+            arrive(att_stat.at[k], att_sems, k, (k, tp))
+            arrive(att_value.at[k], att_sems, K + k, (k, tp))
+        highs, sums = [own_score], [jnp.ones((N, 1), jnp.float32)]
+        for k in range(K):
+            stat = wide(att_stat[k])
+            highs.append(jnp.sum(jnp.where(high_at, stat, 0.0), axis=-1, keepdims=True))
+            sums.append(jnp.sum(jnp.where(total_at, stat, 0.0), axis=-1, keepdims=True))
+        top = highs[0]
+        for h in highs[1:]:
+            top = jnp.maximum(top, h)
+        shrink = [jnp.exp(h - top) for h in highs]
+        accum = own_value * shrink[0]
+        denom = shrink[0]
+        for k in range(K):
+            accum = accum + att_value[k].astype(jnp.float32) * shrink[k + 1]
+            denom = denom + sums[k + 1] * shrink[k + 1]
+        ratio_rows[...] = accum / denom
+        heads = []
+        for g in range(groups):
+            first = ratio_rows[pl.ds(g * 2, B, stride=R), :]
+            second = ratio_rows[pl.ds(g * 2 + 1, B, stride=R), :]
+            mixed = first - lam_ref[g] * second
+            scale = lax.rsqrt(jnp.mean(mixed * mixed, axis=-1, keepdims=True) + epsilon)
+            heads.append((mixed * scale * hgain[...]).astype(jnp.bfloat16))
+        heads_out = jnp.concatenate(heads, axis=1)
+        out_parts[tp] = jnp.dot(heads_out, wo[...], preferred_element_type=jnp.float32)
+        for dt in range(1, T):
+            sent.append(send(out_parts.at[tp], out_parts.at[tp], out_sems, dt, tp, at(0, dt)))
+        for dt in range(1, T):
+            _, t = at(0, dt)
+            arrive(out_parts.at[t], out_sems, t, (kv, t))
+        mixer = out_parts[0]
+        for t in range(1, T):
+            mixer = mixer + out_parts[t]
+        rows_two[kv] = (stream[...] + mixer).astype(jnp.bfloat16)
+        for dk in kv_offsets[:-1]:
+            sent.append(
+                send(rows_two.at[kv], rows_two.at[kv], two_rows_sems, dk, kv, at(dk, 0))
+            )
+        loads["gate1"].wait()
+        loads["up1"].wait()
+        loads["down1"].wait()
+        for dk in kv_offsets[:-1]:
+            k, _ = at(dk, 0)
+            arrive(rows_two.at[k], two_rows_sems, k, (k, tp))
+    with jax.named_scope("half_two"):
+        hidden = hidden_of(jnp.concatenate([rows_two[k] for k in range(K)], axis=1), 2, 1)
+        for dk in kv_offsets:
+            k, _ = at(dk, 0)
+            part = down_block(hidden, 1, k).astype(SUM_TWO)
+            for t in range(T):
+                send_two[dk, t] = part[:, t * C : (t + 1) * C]
+            for dt in range(T):
+                _, t = at(0, dt)
+                if (dk, dt) != (0, 0):
+                    sent.append(
+                        send(
+                            send_two.at[dk, t], recv_two.at[me], two_sems, dk * T + dt, me, (k, t)
+                        )
+                    )
+        recv_two[me] = send_two[0, tp]
+        base = rows_two[kv, :, pl.ds(pl.multiple_of(tp * C, C), C)].astype(jnp.float32)
+        for dk, dt in peers:
+            k, t = at(dk, dt)
+            arrive(recv_two.at[k * T + t], two_sems, k * T + t, (k, t))
+        summed = recv_two[0].astype(jnp.float32)
+        for g in range(1, G):
+            summed = summed + recv_two[g].astype(jnp.float32)
+        out_ref[...] = (base + summed).astype(jnp.bfloat16)
+        for copy in sent:
+            copy.wait_send()
+
+
+def fits(args, K, T):
+    residual, gate, query, key, value = args[0], args[2], args[5], args[6], args[7]
+    B, C = residual.shape
+    heads = query.shape[1] // (2 * HEAD)
+    return (
+        B == 8
+        and C % 128 == 0
+        and query.shape[0] == T * C
+        and gate.shape[1] % 16 == 0
+        and key.shape[1] == 2 * HEAD
+        and value.shape[1] == VDIM
+        and heads * 2 == 8
+        and args[11].shape[1] % 128 == 0
+    )
+
+
+def local_fused(K, T, *args):
+    if not fits(args, K, T):
+        return local(*args)
+    (
+        residual,
+        norm_gains,
+        ffn_gate,
+        ffn_up,
+        ffn_down,
+        proj_query,
+        proj_key,
+        proj_value,
+        proj_out,
+        head_lambda,
+        head_gain,
+        cache_keys,
+        cache_values,
+        live_length,
+    ) = args
+    B, C = residual.shape
+    G, W = K * T, T * C
+    span = cache_keys.shape[1]
+    bf16, f32 = jnp.bfloat16, jnp.float32
+    NQ, NK, NV = proj_query.shape[1], proj_key.shape[1], proj_value.shape[1]
+    N = B * 2 * (NQ // NK)
+    cache_keys = cache_keys.reshape(B, span, NK)
+    cache_values = cache_values.reshape(B, span, NV)
+    head_gain = head_gain.reshape(1, NV)
+    like = lambda a: pltpu.VMEM(a.shape, a.dtype)
+    dma = lambda n: pltpu.SemaphoreType.DMA((2, n))
+    return pl.pallas_call(
+        functools.partial(fused_kernel, K, T),
+        out_shape=pltpu.VMEM((B, C), bf16),
+        in_specs=[pl.BlockSpec(memory_space=pl.ANY)] * 14,
+        out_specs=pl.BlockSpec(memory_space=pltpu.VMEM),
+        scratch_shapes=[
+            like(norm_gains),
+            like(ffn_gate),
+            like(ffn_up),
+            like(ffn_down),
+            like(proj_query),
+            like(proj_key),
+            like(proj_value),
+            like(proj_out),
+            like(head_gain),
+            like(cache_keys),
+            like(cache_values),
+            pltpu.VMEM((G, B, C), bf16),
+            pltpu.VMEM((K, B, W), SUM_ONE),
+            pltpu.VMEM((G, B, W), SUM_ONE),
+            pltpu.VMEM((B, W), f32),
+            pltpu.VMEM((K, B, NQ + NK + NV + 128), f32),
+            pltpu.VMEM((N, NK), f32),
+            pltpu.VMEM((K, N, NV), ATT_TYPE),
+            pltpu.VMEM((K, B, 128), f32),
+            pltpu.VMEM((N, NV), f32),
+            pltpu.VMEM((T, B, W), f32),
+            pltpu.VMEM((K, B, W), bf16),
+            pltpu.VMEM((K, T, B, C), SUM_TWO),
+            pltpu.VMEM((G, B, C), SUM_TWO),
+            pltpu.SemaphoreType.DMA((17,)),
+            dma(G),
+            dma(G),
+            dma(K),
+            dma(2 * K),
+            dma(T),
+            dma(K),
+            dma(G),
+            pltpu.SMEM(head_lambda.shape, f32),
+            pltpu.SMEM(live_length.shape, jnp.int32),
+        ],
+        compiler_params=pltpu.CompilerParams(
+            collective_id=0, has_side_effects=True, vmem_limit_bytes=56 << 20
+        ),
+    )(
+        head_lambda,
+        live_length,
+        residual,
+        norm_gains,
+        ffn_gate,
+        ffn_up,
+        ffn_down,
+        proj_query,
+        proj_key,
+        proj_value,
+        proj_out,
+        head_gain,
+        cache_keys,
+        cache_values,
+    )
+
+
 def solution(mesh):
     in_specs = (
         P("dp", ("kv", "tp")),
@@ -149,4 +605,5 @@
         P("dp"),
     )
     out_specs = P("dp", ("kv", "tp"))
-    return jax.shard_map(local, mesh=mesh, in_specs=in_specs, out_specs=out_specs, check_vma=False)
+    body = functools.partial(local_fused, mesh.shape["kv"], mesh.shape["tp"])
+    return jax.shard_map(body, mesh=mesh, in_specs=in_specs, out_specs=out_specs, check_vma=False)

time: 196 us -> 36.1 us (0.18)
  blocking collectives: 87.6 us -> 0 us
  waiting for transfers between devices: 69.9 us -> 0 us
  Pallas kernels: 0 us -> 35.3 us
  matrix products: 17.3 us -> 0 us
  between operations: 13.3 us -> 0.01 us
  other arithmetic: 4.66 us -> 0 us
  local copies, waits for them, and re-layouts: 3.08 us -> 0.6 us
    all_gather x6 -> x0, blocking collectives: 71.8 us -> none  [the longest x3 39.6 us: joined(): gathered = jax.tree.map(lambda a: lax.all_gather(a, axis), part)]
    reduce_scatter x3 -> x0, waiting for transfers between devices: 69.8 us -> none  [the longest x1 31.5 us: local(): lax.psum_scatter(term_two, ('kv', 'tp'), scatter_dimension=1, tiled=True)]
    pallas_call x0 -> x1, Pallas kernels: none -> 35.3 us  [local_fused(): pl.pallas_call(functools.partial(fused_kernel, K, T), out_shape=pltpu.VME...]
    dot_general x11 -> x0, matrix products: 17.3 us -> none  [the longest x2 10 us: channel_mix(): return 0.5 * jnp.dot(hidden, down_part, preferred_element_type=jnp.float32)]
    psum x1 -> x0, blocking collectives: 15.8 us -> none  [local(): lax.psum((query_part, key_part, value_part, squares), 'kv')]
    convert_element_type x5 -> x0, other arithmetic: 2.84 us -> none  [the longest x1 1.29 us: local(): return (stream_two.astype(jnp.float32) + summed_two).astype(jnp.bfloat16)]
  transfers between devices with their start and end apart: 3 -> 0, of which waited for: 3 -> 0; matrix products, arithmetic and copies ran while one was open for 0% -> 0% of each run, Pallas kernels for 0% -> 0%
where the time goes in v1:
time: 36.1 us; the launch traced here: 35.9 us
  Pallas kernels  35.3 us (98%)
  local copies, waits for them, and re-layouts  0.6 us (2%)
    pallas_call x1, Pallas kernels, local_fused(): pl.pallas_call(functools.partial(fused_kernel, K, T), out_shape=pltpu.VME...  35.3 us

profile of v1, /device:TPU:0, one launch (start us, length us, event | category | flops | bytes accessed | tf_op | source)
XLA Modules:
  0.0 35.9 jit_solution(2432777437210552606)
XLA Ops:
  0.0 35.3 %shard_map.136 = bf16[8,256]{1,0:T(8,128)(2,1)S(1)} custom-call(f32[4]{0:T(128)} %head_lambda.1, s32[8]{0:T(128)} %live_length.1, bf16[8,256]{1,0:T(8,128)(2,1)} %residual.1, f32[3,2048]{1,0:T(4,128)} %norm_gains.1, bf16[2,704,2048]{2,1,0:T(8,128)(2,1)} %ffn_gate.1, bf16[2,704,2048]{2,1,0:T(8,128)(2,1)} %ffn_up.1, bf16[2,704,2048]{2,1,0:T(8,128)(2,1)} %ffn_down.1, ...), custom_call_target="tpu_custom_call" | custom-call | tf_op jit(solution)/shard_map/pallas_call | solution.py:528
  35.3 0.6 %copy.16 = bf16[8,256]{1,0:T(8,128)(2,1)} copy(bf16[8,256]{1,0:T(8,128)(2,1)S(1)} %shard_map.136) | data formatting | bytes 8192

commit v2 on v1

--- a/solution.py
+++ b/solution.py
@@ -139,7 +139,7 @@
 NT = (((1,), (1,)), ((), ()))
 SUM_ONE = jnp.float32
 SUM_TWO = jnp.bfloat16
-ATT_TYPE = jnp.float32
+ATT_TYPE = jnp.bfloat16
 
 
 def fused_kernel(
@@ -202,8 +202,15 @@
     W = T * C
     width = G * C
 
+    upper = lax.rem(kv * 2 // K, 2)
+
     def at(dk, dt):
-        return lax.rem(kv + dk, K), lax.rem(tp + dt, T)
+        if dk == 0:
+            return kv, lax.rem(tp + dt, T)
+        low, high = dk - 1, K - dk
+        rising = low + (low + K - kv) // K
+        falling = high - (kv - high + K) // K
+        return upper * rising + (1 - upper) * falling, lax.rem(tp + dt, T)
 
     def send(src, dst, sems, lane, slot, place):
         copy = pltpu.make_async_remote_copy(
@@ -237,7 +244,7 @@
 
     load("rows", residual, rows_one.at[me])
     barrier = pltpu.get_barrier_semaphore()
-    kv_offsets = sorted(range(1, K), key=lambda dk: abs(2 * dk - K)) + [0]
+    kv_offsets = [*range(1, K), 0]
     offsets = [(dk, dt) for dk in kv_offsets for dt in range(T)]
     peers = [o for o in offsets if o != (0, 0)]
     for dk, dt in peers:

time: 36.1 us -> 34.6 us (0.958)
  Pallas kernels: 35.3 us -> 33.8 us
    pallas_call x1, Pallas kernels: 35.3 us -> 33.8 us  [local_fused(): pl.pallas_call(functools.partial(fused_kernel, K, T), out_shape=pltpu.VME...]
where the time goes in v2:
time: 34.6 us; the launch traced here: 34.4 us
  Pallas kernels  33.8 us (98%)
  local copies, waits for them, and re-layouts  0.6 us (2%)
    pallas_call x1, Pallas kernels, local_fused(): pl.pallas_call(functools.partial(fused_kernel, K, T), out_shape=pltpu.VME...  33.8 us

profile of v2, /device:TPU:0, one launch (start us, length us, event | category | flops | bytes accessed | tf_op | source)
XLA Modules:
  0.0 34.4 jit_solution(5426190402674644604)
XLA Ops:
  0.0 33.8 %shard_map.136 = bf16[8,256]{1,0:T(8,128)(2,1)S(1)} custom-call(f32[4]{0:T(128)} %head_lambda.1, s32[8]{0:T(128)} %live_length.1, bf16[8,256]{1,0:T(8,128)(2,1)} %residual.1, f32[3,2048]{1,0:T(4,128)} %norm_gains.1, bf16[2,704,2048]{2,1,0:T(8,128)(2,1)} %ffn_gate.1, bf16[2,704,2048]{2,1,0:T(8,128)(2,1)} %ffn_up.1, bf16[2,704,2048]{2,1,0:T(8,128)(2,1)} %ffn_down.1, ...), custom_call_target="tpu_custom_call" | custom-call | tf_op jit(solution)/shard_map/pallas_call | solution.py:535
  33.8 0.6 %copy.16 = bf16[8,256]{1,0:T(8,128)(2,1)} copy(bf16[8,256]{1,0:T(8,128)(2,1)S(1)} %shard_map.136) | data formatting | bytes 8192

commit v3 on v2

--- a/solution.py
+++ b/solution.py
@@ -194,6 +194,9 @@
     two_sems,
     lam_ref,
     len_ref,
+    square_sums,
+    own_parts,
+    own_sems,
 ):
     kv, tp = lax.axis_index("kv"), lax.axis_index("tp")
     G = K * T
@@ -326,17 +329,39 @@
         gain_block = gains[1:2, pl.ds(pl.multiple_of(kv * W, W), W)]
         scaled = (one32 * gain_block).astype(jnp.bfloat16)
         NQ, NK, NV = wq.shape[1], wk.shape[1], wv.shape[1]
-        qkv[kv] = jnp.concatenate(
+        diagonal = lax.broadcasted_iota(jnp.int32, (B, 128), 0) == lax.broadcasted_iota(
+            jnp.int32, (B, 128), 1
+        )
+        square_sums[kv] = jnp.sum(jnp.where(diagonal, squares, 0.0), axis=0, keepdims=True)
+        qkv[kv] = jnp.dot(scaled, wq[...], preferred_element_type=jnp.float32)
+        for dk in kv_offsets[:-1]:
+            sent.append(send(qkv.at[kv], qkv.at[kv], qkv_sems, dk, kv, at(dk, 0)))
+            sent.append(
+                send(square_sums.at[kv], square_sums.at[kv], qkv_sems, K + dk, K + kv, at(dk, 0))
+            )
+        own_parts[kv] = jnp.concatenate(
             [
-                jnp.dot(scaled, wq[...], preferred_element_type=jnp.float32),
                 jnp.dot(scaled, wk[...], preferred_element_type=jnp.float32),
                 jnp.dot(scaled, wv[...], preferred_element_type=jnp.float32),
-                jnp.broadcast_to(squares, (B, 128)),
             ],
             axis=1,
         )
-        for dk in kv_offsets[:-1]:
-            sent.append(send(qkv.at[kv], qkv.at[kv], qkv_sems, dk, kv, at(dk, 0)))
+        owner = lax.rem(K // 2 + K - 1 + tp, K)
+
+        def own_copy(k):
+            return pltpu.make_async_remote_copy(
+                src_ref=own_parts.at[k],
+                dst_ref=own_parts.at[k],
+                send_sem=own_sems.at[0, 0],
+                recv_sem=own_sems.at[1, k],
+                device_id={"kv": owner, "tp": tp},
+                device_id_type=MESH,
+            )
+
+        @pl.when(kv != owner)
+        def _():
+            own_copy(kv).start()
+
         loads["keys"].wait()
         loads["values"].wait()
         loads["lam"].wait()
@@ -346,15 +371,17 @@
         for dk in kv_offsets[:-1]:
             k, _ = at(dk, 0)
             arrive(qkv.at[k], qkv_sems, k, (k, tp))
+            arrive(square_sums.at[k], qkv_sems, K + k, (k, tp))
     with jax.named_scope("attend"):
         total = qkv[0]
         for k in range(1, K):
             total = total + qkv[k]
-        factor = lax.rsqrt(total[:, NQ + NK + NV : NQ + NK + NV + 1] / width + epsilon)
-        queries = (total[:, :NQ] * factor).astype(jnp.bfloat16).astype(jnp.float32)
-        key_new = (total[:, NQ : NQ + NK] * factor).astype(jnp.bfloat16).astype(jnp.float32)
-        value_new = (total[:, NQ + NK : NQ + NK + NV] * factor).astype(jnp.bfloat16)
-        value_new = value_new.astype(jnp.float32)
+        square_row = square_sums[0]
+        for k in range(1, K):
+            square_row = square_row + square_sums[k]
+        square_sum = jnp.sum(jnp.where(diagonal, square_row, 0.0), axis=-1, keepdims=True)
+        factor = lax.rsqrt(square_sum / width + epsilon)
+        queries = (total * factor).astype(jnp.bfloat16).astype(jnp.float32)
         groups = NQ // NK
         R = 2 * groups
         lane = lax.broadcasted_iota(jnp.int32, (B, NK), 1)
@@ -395,27 +422,47 @@
         lanes = lax.broadcasted_iota(jnp.int32, (N, 128), 1)
         place = lax.rem(lax.broadcasted_iota(jnp.int32, (N, 128), 0), R)
         high_at, total_at = lanes == place, lanes == place + R
-        packed = jnp.where(high_at, highest, jnp.where(total_at, totals, 0.0))
-        att_stat[kv] = jnp.sum(packed.reshape(B, R, 128), axis=1)
-        att_value[kv] = jnp.concatenate(weighted, axis=0).astype(ATT_TYPE)
+
+        def wide(a):
+            return jnp.broadcast_to(a[:, None, :], (B, R, a.shape[1])).reshape(N, a.shape[1])
+
+        def put(high, total, value):
+            packed = jnp.where(high_at, high, jnp.where(total_at, total, 0.0))
+            att_stat[kv] = jnp.sum(packed.reshape(B, R, 128), axis=1)
+            att_value[kv] = value.astype(ATT_TYPE)
+
+        block_value = jnp.concatenate(weighted, axis=0)
+
+        @pl.when(kv != owner)
+        def _():
+            put(highest, totals, block_value)
+
+        @pl.when(kv == owner)
+        def _():
+            for dk in kv_offsets[:-1]:
+                k, _ = at(dk, 0)
+                arrive(own_parts.at[k], own_sems, k, (k, tp))
+            own = own_parts[0]
+            for k in range(1, K):
+                own = own + own_parts[k]
+            own = (own * factor).astype(jnp.bfloat16).astype(jnp.float32)
+            own_score = score_scale * jnp.sum(
+                jnp.concatenate(q_all, axis=0) * wide(own[:, :NK]), axis=-1, keepdims=True
+            )
+            top = jnp.maximum(highest, own_score)
+            early, late = jnp.exp(highest - top), jnp.exp(own_score - top)
+            put(top, totals * early + late, block_value * early + wide(own[:, NK:]) * late)
+
         for dk in kv_offsets[:-1]:
             sent.append(send(att_stat.at[kv], att_stat.at[kv], att_sems, dk, kv, at(dk, 0)))
             sent.append(
                 send(att_value.at[kv], att_value.at[kv], att_sems, K + dk, K + kv, at(dk, 0))
             )
-
-        def wide(a):
-            return jnp.broadcast_to(a[:, None, :], (B, R, a.shape[1])).reshape(N, a.shape[1])
-
-        own_score = jnp.sum(
-            jnp.concatenate(q_all, axis=0) * wide(key_new), axis=-1, keepdims=True
-        ) * score_scale
-        own_value = wide(value_new)
         for dk in kv_offsets[:-1]:
             k, _ = at(dk, 0)
             arrive(att_stat.at[k], att_sems, k, (k, tp))
             arrive(att_value.at[k], att_sems, K + k, (k, tp))
-        highs, sums = [own_score], [jnp.ones((N, 1), jnp.float32)]
+        highs, sums = [], []
         for k in range(K):
             stat = wide(att_stat[k])
             highs.append(jnp.sum(jnp.where(high_at, stat, 0.0), axis=-1, keepdims=True))
@@ -424,11 +471,11 @@
         for h in highs[1:]:
             top = jnp.maximum(top, h)
         shrink = [jnp.exp(h - top) for h in highs]
-        accum = own_value * shrink[0]
-        denom = shrink[0]
-        for k in range(K):
-            accum = accum + att_value[k].astype(jnp.float32) * shrink[k + 1]
-            denom = denom + sums[k + 1] * shrink[k + 1]
+        accum = att_value[0].astype(jnp.float32) * shrink[0]
+        denom = sums[0] * shrink[0]
+        for k in range(1, K):
+            accum = accum + att_value[k].astype(jnp.float32) * shrink[k]
+            denom = denom + sums[k] * shrink[k]
         ratio_rows[...] = accum / denom
         heads = []
         for g in range(groups):
@@ -485,6 +532,10 @@
         for copy in sent:
             copy.wait_send()
 
+        @pl.when(kv != owner)
+        def _():
+            own_copy(kv).wait_send()
+
 
 def fits(args, K, T):
     residual, gate, query, key, value = args[0], args[2], args[5], args[6], args[7]
@@ -553,7 +604,7 @@
             pltpu.VMEM((K, B, W), SUM_ONE),
             pltpu.VMEM((G, B, W), SUM_ONE),
             pltpu.VMEM((B, W), f32),
-            pltpu.VMEM((K, B, NQ + NK + NV + 128), f32),
+            pltpu.VMEM((K, B, NQ), f32),
             pltpu.VMEM((N, NK), f32),
             pltpu.VMEM((K, N, NV), ATT_TYPE),
             pltpu.VMEM((K, B, 128), f32),
@@ -565,13 +616,16 @@
             pltpu.SemaphoreType.DMA((17,)),
             dma(G),
             dma(G),
-            dma(K),
+            dma(2 * K),
             dma(2 * K),
             dma(T),
             dma(K),
             dma(G),
             pltpu.SMEM(head_lambda.shape, f32),
             pltpu.SMEM(live_length.shape, jnp.int32),
+            pltpu.VMEM((K, 1, 128), f32),
+            pltpu.VMEM((K, B, NK + NV), f32),
+            dma(K),
         ],
         compiler_params=pltpu.CompilerParams(
             collective_id=0, has_side_effects=True, vmem_limit_bytes=56 << 20

time: 34.6 us -> 34 us (0.983)
  Pallas kernels: 33.8 us -> 33.3 us
    pallas_call x1, Pallas kernels: 33.8 us -> 33.3 us  [local_fused(): pl.pallas_call(functools.partial(fused_kernel, K, T), out_shape=pltpu.VME...]
where the time goes in v3:
time: 34 us; the launch traced here: 33.9 us
  Pallas kernels  33.3 us (98%)
  local copies, waits for them, and re-layouts  0.6 us (2%)
    pallas_call x1, Pallas kernels, local_fused(): pl.pallas_call(functools.partial(fused_kernel, K, T), out_shape=pltpu.VME...  33.3 us

profile of v3, /device:TPU:0, one launch (start us, length us, event | category | flops | bytes accessed | tf_op | source)
XLA Modules:
  0.0 33.9 jit_solution(4716597268229657350)
XLA Ops:
  0.0 33.3 %shard_map.136 = bf16[8,256]{1,0:T(8,128)(2,1)S(1)} custom-call(f32[4]{0:T(128)} %head_lambda.1, s32[8]{0:T(128)} %live_length.1, bf16[8,256]{1,0:T(8,128)(2,1)} %residual.1, f32[3,2048]{1,0:T(4,128)} %norm_gains.1, bf16[2,704,2048]{2,1,0:T(8,128)(2,1)} %ffn_gate.1, bf16[2,704,2048]{2,1,0:T(8,128)(2,1)} %ffn_up.1, bf16[2,704,2048]{2,1,0:T(8,128)(2,1)} %ffn_down.1, ...), custom_call_target="tpu_custom_call" | custom-call | tf_op jit(solution)/shard_map/pallas_call | solution.py:586
  33.3 0.6 %copy.16 = bf16[8,256]{1,0:T(8,128)(2,1)} copy(bf16[8,256]{1,0:T(8,128)(2,1)S(1)} %shard_map.136) | data formatting | bytes 8192
